TPU v7x, 32 devices: a whole 2x2x4 slice. The times are simulated.
32 devices in a mesh: sp: 8 (over z, y), tp: 4 (over x, core).
Axes of the slice: x: 2, y: 2, z: 4, core: 2. Of those that a mesh axis runs over, the one named last changes fastest.
Arguments:
- tokens: bfloat16 [2048, 2048], P('sp'), may hold values from -72 to 72
- query_weight: bfloat16 [3, 2048, 1024], P(None, None, 'tp'), may hold values from -0.125 to 0.125
- key_weight: bfloat16 [3, 2048, 1024], P(None, None, 'tp'), may hold values from -0.125 to 0.125
- value_weight: bfloat16 [3, 2048, 1024], P(None, None, 'tp'), may hold values from -0.125 to 0.125
- out_weight: bfloat16 [1024, 2048], P(None, 'tp'), may hold values from -2 to 2
Outputs:
- mixed: bfloat16 [2048, 2048], P('sp', 'tp')
All inputs are finite; a program needn't handle non-finite values.
Results may differ from a plain program's by a relative error of at most 0.012.
Values may be sent and summed in bfloat16 or wider, within the bound.
A program may use at most 64 MiB of HBM per device.

v0:
```python
import math
import jax
import jax.numpy as jnp
from jax import lax
from jax.sharding import PartitionSpec as P

HEAD_DIM = 64
SIDE_STEPS = 64
MIDDLE_DILATION = 4
FAR_DILATION = 16


def shifted(block, axis, distance):
    devices = range(lax.axis_size(axis))
    route = [(i - distance, i) for i in devices if i - distance in devices]
    return lax.ppermute(block, axis, route)


def with_halo(block, sides, width):
    for axis, dim in sides:
        count = lax.axis_size(axis)
        forward = [(i, i + 1) for i in range(count - 1)]
        backward = [(target, source) for source, target in forward]
        low = lax.ppermute(
            lax.slice_in_dim(block, block.shape[dim] - width, None, axis=dim), axis, forward
        )
        high = lax.ppermute(lax.slice_in_dim(block, 0, width, axis=dim), axis, backward)
        block = jnp.concatenate([low, block, high], axis=dim)
    return block


def rotate(projected, offset_pos):
    length, columns = projected.shape
    heads = columns // HEAD_DIM
    half = HEAD_DIM // 2
    positions = (offset_pos + jnp.arange(length)).astype(jnp.float32)
    inverse = 1.0 / 10000.0 ** (jnp.arange(half, dtype=jnp.float32) * 2.0 / HEAD_DIM)
    angles = positions[:, None] * inverse[None, :]
    angles = jnp.concatenate([angles, angles], axis=-1)
    cosine_table = jnp.cos(angles)[:, None, :]
    sine = jnp.sin(angles)[:, None, :]
    shaped = projected.reshape(length, heads, HEAD_DIM)
    turned = jnp.concatenate([-shaped[..., half:], shaped[..., :half]], axis=-1)
    return (shaped * cosine_table + turned * sine).reshape(length, columns)


def banded(queries, key_ext, value_ext, dilation, offset_pos, seq_len):
    length, columns = queries.shape
    heads = columns // HEAD_DIM
    class_len = length // dilation
    block_len = math.gcd(SIDE_STEPS, class_len)
    blocks = class_len // block_len
    extra = 2 * SIDE_STEPS // block_len
    query_blocks = queries.reshape(blocks, block_len, dilation, heads, HEAD_DIM)
    key_blocks = key_ext.reshape(blocks + extra, block_len, dilation, heads, HEAD_DIM)
    value_blocks = value_ext.reshape(blocks + extra, block_len, dilation, heads, HEAD_DIM)
    key_win = jnp.concatenate(
        [key_blocks[shift_idx : shift_idx + blocks] for shift_idx in range(extra + 1)], axis=1
    )
    value_win = jnp.concatenate(
        [value_blocks[shift_idx : shift_idx + blocks] for shift_idx in range(extra + 1)], axis=1
    )
    scores = jnp.einsum(
        "bqrhe,bkrhe->brhqk", query_blocks, key_win, preferred_element_type=jnp.float32
    )
    scores = scores * HEAD_DIM ** (-0.5)
    width_keys = key_win.shape[1]
    relative = jnp.arange(width_keys)[None, :] - jnp.arange(block_len)[:, None]
    within = (relative >= 0) & (relative <= 2 * SIDE_STEPS)
    key_rows = jnp.arange(blocks)[:, None] * block_len + jnp.arange(width_keys)[None, :]
    spots = (
        offset_pos
        - SIDE_STEPS * dilation
        + dilation * key_rows[:, :, None]
        + jnp.arange(dilation)[None, None, :]
    )
    inside = (spots >= 0) & (spots < seq_len)
    allowed = within[None, None, None] & jnp.transpose(inside, (0, 2, 1))[:, :, None, None, :]
    scores = jnp.where(allowed, scores, -1e30)
    row_max = jnp.max(scores, axis=-1, keepdims=True)
    expo = jnp.exp(scores - row_max)
    denom = jnp.sum(expo, axis=-1)
    probs = expo.astype(jnp.bfloat16)
    summed = jnp.einsum("brhqk,bkrhe->bqrhe", probs, value_win, preferred_element_type=jnp.float32)
    group_out = summed / jnp.transpose(denom, (0, 3, 1, 2))[..., None]
    log_sum = row_max[..., 0] + jnp.log(denom)
    log_sum = jnp.transpose(log_sum, (0, 3, 1, 2)).reshape(length, heads)
    return (group_out.reshape(length, columns), log_sum)


def collect(own_block, needed, direction):
    collected = own_block[None]
    while collected.shape[0] < needed + 1:
        stride = collected.shape[0]
        to_send = min(stride, needed + 1 - stride)
        arrived = shifted(collected[:to_send], "sp", direction * stride)
        collected = jnp.concatenate([collected, arrived], axis=0)
    return collected[1:]


def per_device(tokens, query_weight, key_weight, value_weight, out_weight):
    length = tokens.shape[0]
    offset_pos = lax.axis_index("sp") * length
    seq_len = lax.axis_size("sp") * length
    group_dilations = (1, MIDDLE_DILATION, FAR_DILATION)
    query_list = []
    pairs = []
    for group_idx in range(3):
        queries = rotate(
            jnp.dot(tokens, query_weight[group_idx], preferred_element_type=jnp.float32), offset_pos
        )
        keys_here = rotate(
            jnp.dot(tokens, key_weight[group_idx], preferred_element_type=jnp.float32), offset_pos
        )
        values_here = jnp.dot(tokens, value_weight[group_idx], preferred_element_type=jnp.float32)
        query_list.append(queries.astype(jnp.bfloat16))
        pairs.append(
            jnp.stack([keys_here.astype(jnp.bfloat16), values_here.astype(jnp.bfloat16)], axis=0)
        )
    middle_span_length = SIDE_STEPS * MIDDLE_DILATION
    first_ext = with_halo(pairs[0], (("sp", 1),), SIDE_STEPS)
    middle_ext = with_halo(pairs[1], (("sp", 1),), middle_span_length)
    far_span_length = SIDE_STEPS * FAR_DILATION
    needed = -(-far_span_length // length)
    lower_blocks = collect(pairs[2], needed, 1)
    upper_blocks = collect(pairs[2], needed, -1)
    columns = pairs[2].shape[2]
    lower_flat = jnp.moveaxis(lower_blocks[::-1], 0, 1).reshape(2, needed * length, columns)
    upper_flat = jnp.moveaxis(upper_blocks, 0, 1).reshape(2, needed * length, columns)
    far_full = jnp.concatenate([lower_flat, pairs[2], upper_flat], axis=1)
    extended = (first_ext, middle_ext, far_full)
    outputs = []
    log_sums = []
    for group_idx in range(3):
        group_out, log_sum = banded(
            query_list[group_idx],
            extended[group_idx][0],
            extended[group_idx][1],
            group_dilations[group_idx],
            offset_pos,
            seq_len,
        )
        outputs.append(group_out)
        log_sums.append(log_sum)
    merge_w = jax.nn.softmax(jnp.stack(log_sums, axis=0), axis=0)
    heads = columns // HEAD_DIM
    stacked = jnp.stack(outputs, axis=0).reshape(3, length, heads, HEAD_DIM)
    merged = (
        jnp.sum(merge_w[..., None] * stacked, axis=0).reshape(length, columns).astype(jnp.bfloat16)
    )
    mixed = jnp.dot(
        lax.all_gather(merged, "tp", axis=1, tiled=True),
        out_weight,
        preferred_element_type=jnp.float32,
    )
    return mixed.astype(jnp.bfloat16)


def solution(mesh):
    placed = (
        P("sp", None),
        P(None, None, "tp"),
        P(None, None, "tp"),
        P(None, None, "tp"),
        P(None, "tp"),
    )
    return jax.shard_map(
        per_device, mesh=mesh, in_specs=placed, out_specs=P("sp", "tp"), check_vma=False
    )
```

profile of v0, /device:TPU:13, one launch (start us, length us, event | category | flops | bytes accessed | tf_op | source)
XLA Modules:
  0.0 186.6 jit_solution(4766220064842487170)
XLA Ops:
  0.0 3.1 %slice_bitcast_fusion.4 = (bf16[256,2048]{0,1:T(8,128)(2,1)S(1)}, bf16[256,2048]{0,1:T(8,128)(2,1)}, bf16[256,2048]{0,1:T(8,128)(2,1)S(1)}) fusion(bf16[3,2048,256]{2,1,0:T(8,128)(2,1)} %param.7), kind=kLoop, calls=%fused_computation.45 | loop fusion | bytes 6291456 | tf_op jit(solution)/shard_map/dot_general | solution.py:113
  3.1 2.3 %copy.111 = bf16[256,2048]{1,0:T(8,128)(2,1)} copy(bf16[256,2048]{0,1:T(8,128)(2,1)} %get-tuple-element.9) | data formatting | bytes 2097152 | tf_op jit(solution)/shard_map/dot_general | solution.py:113
  7.1 1.7 fusion.18
  12.4 1.8 maximum_bitcast_fusion.9
  14.2 4.9 %collective-permute-start.6 = (bf16[1,2,256,256]{3,2,1,0:T(8,128)(2,1)}, bf16[1,2,256,256]{3,2,1,0:T(8,128)(2,1)}, u32[]{:S(2)}, u32[]{:S(2)}) collective-permute-start(bf16[1,2,256,256]{3,2,1,0:T(8,128)(2,1)} %maximum_bitcast_fusion.9), channel_id=1, source_target_pairs={{0,16},{4,20},{8,24},{12,28},{1,17},{5,21},{9,25},{13,29},{2,18},{... | collective-permute-start | bytes 786440 | tf_op jit(solution)/shard_map/ppermute | solution.py:16
  19.1 2.1 %collective-permute-start.7 = (bf16[1,2,256,256]{3,2,1,0:T(8,128)(2,1)}, bf16[1,2,256,256]{3,2,1,0:T(8,128)(2,1)}, u32[]{:S(2)}, u32[]{:S(2)}) collective-permute-start(bf16[1,2,256,256]{3,2,1,0:T(8,128)(2,1)} %maximum_bitcast_fusion.9), channel_id=1, source_target_pairs={{4,0},{8,4},{12,8},{16,12},{20,16},{24,20},{28,24},{5,1},{9,5},{13... | collective-permute-start | bytes 786440 | tf_op jit(solution)/shard_map/ppermute | solution.py:16
  21.2 4.0 %collective-permute-start.4 = (bf16[1,2,256,256]{3,2,1,0:T(8,128)(2,1)}, bf16[1,2,256,256]{3,2,1,0:T(8,128)(2,1)}, u32[]{:S(2)}, u32[]{:S(2)}) collective-permute-start(bf16[1,2,256,256]{3,2,1,0:T(8,128)(2,1)} %maximum_bitcast_fusion.9), channel_id=1, source_target_pairs={{0,4},{4,8},{8,12},{12,16},{16,20},{20,24},{24,28},{1,5},{5,9},{9,... | collective-permute-start | bytes 786440 | tf_op jit(solution)/shard_map/ppermute | solution.py:16
  28.6 2.3 %copy.91 = bf16[256,2048]{1,0:T(8,128)(2,1)} copy(bf16[256,2048]{0,1:T(8,128)(2,1)} %get-tuple-element.5) | data formatting | bytes 2097152 | tf_op jit(solution)/shard_map/dot_general | solution.py:110
  30.9 1.7 fusion.28
  34.0 2.3 %copy.99 = bf16[256,2048]{1,0:T(8,128)(2,1)} copy(bf16[256,2048]{0,1:T(8,128)(2,1)} %get-tuple-element.7) | data formatting | bytes 2097152 | tf_op jit(solution)/shard_map/dot_general | solution.py:110
  36.3 2.4 %fusion.24 = f32[256,4,64]{0,2,1:T(8,128)} fusion(bf16[4,64,2048]{2,1,0:T(8,128)(2,1)} %bitcast.222, bf16[256,2048]{1,0:T(8,128)(2,1)S(1)} %copy-done), kind=kOutput, calls=%fused_computation.28 | convolution fusion | flops 268435456 | bytes 2359296 | tf_op jit(solution)/shard_map/dot_general | solution.py:110
  40.1 2.5 %fusion.26 = f32[256,4,64]{0,2,1:T(8,128)} fusion(bf16[4,64,2048]{2,1,0:T(8,128)(2,1)} %bitcast.223, bf16[256,2048]{1,0:T(8,128)(2,1)S(1)} %copy-done), kind=kOutput, calls=%fused_computation.30 | convolution fusion | flops 268435456 | bytes 2359296 | tf_op jit(solution)/shard_map/dot_general | solution.py:113
  44.0 2.4 %fusion.20 = f32[256,4,64]{0,2,1:T(8,128)} fusion(bf16[4,64,2048]{2,1,0:T(8,128)(2,1)} %bitcast.224, bf16[256,2048]{1,0:T(8,128)(2,1)S(1)} %copy-done), kind=kOutput, calls=%fused_computation.24 | convolution fusion | flops 268435456 | bytes 2359296 | tf_op jit(solution)/shard_map/dot_general | solution.py:110
  50.6 1.9 %collective-permute-start = (bf16[2,64,256]{2,1,0:T(8,128)(2,1)}, bf16[2,64,256]{2,1,0:T(8,128)(2,1)}, u32[]{:S(2)}, u32[]{:S(2)}) collective-permute-start(bf16[2,64,256]{2,1,0:T(8,128)(2,1)} %get-tuple-element.35), channel_id=1, source_target_pairs={{0,4},{4,8},{8,12},{12,16},{16,20},{20,24},{24,28},{1,5},{5,9},{9,... | collective-permute-start | bytes 196616 | tf_op jit(solution)/shard_map/ppermute | solution.py:24
  52.5 3.4 %collective-permute-start.1 = (bf16[2,64,256]{2,1,0:T(8,128)(2,1)}, bf16[2,64,256]{2,1,0:T(8,128)(2,1)}, u32[]{:S(2)}, u32[]{:S(2)}) collective-permute-start(bf16[2,64,256]{2,1,0:T(8,128)(2,1)} %get-tuple-element.36), channel_id=1, source_target_pairs={{4,0},{8,4},{12,8},{16,12},{20,16},{24,20},{28,24},{5,1},{9,5},{13... | collective-permute-start | bytes 196616 | tf_op jit(solution)/shard_map/ppermute | solution.py:27
  71.9 2.3 %collective-permute-start.3 = (bf16[2,256,256]{2,1,0:T(8,128)(2,1)}, bf16[2,256,256]{2,1,0:T(8,128)(2,1)}, u32[]{:S(2)}, u32[]{:S(2)}) collective-permute-start(bf16[2,256,256]{2,1,0:T(8,128)(2,1)} %pad_maximum_fusion.3), channel_id=1, source_target_pairs={{4,0},{8,4},{12,8},{16,12},{20,16},{24,20},{28,24},{5,1},{9,5},{13... | collective-permute-start | bytes 786440 | tf_op jit(solution)/shard_map/ppermute | solution.py:27
  81.0 4.0 %collective-permute-start.2 = (bf16[2,256,256]{2,1,0:T(8,128)(2,1)}, bf16[2,256,256]{2,1,0:T(8,128)(2,1)S(1)}, u32[]{:S(2)}, u32[]{:S(2)}) collective-permute-start(bf16[2,256,256]{2,1,0:T(8,128)(2,1)} %pad_maximum_fusion.3), channel_id=1, source_target_pairs={{0,4},{4,8},{8,12},{12,16},{16,20},{20,24},{24,28},{1,5},{5,9},{9,... | collective-permute-start | bytes 786440 | tf_op jit(solution)/shard_map/ppermute | solution.py:24
  85.0 2.0 %pad_maximum_fusion.1 = (bf16[2,2,256,256]{3,2,1,0:T(8,128)(2,1)S(1)}, bf16[2,2,256,256]{3,2,1,0:T(8,128)(2,1)}) fusion(bf16[1,2,256,256]{3,2,1,0:T(8,128)(2,1)} %maximum_bitcast_fusion.9, bf16[1,2,256,256]{3,2,1,0:T(8,128)(2,1)} %collective-permute-done.7, bf16[1,2,256,256]{3,2,1,0:T(8,128)(2,1)} %collective-permute-done.4), kind=kLoop, calls=%fused_computation.58 | loop fusion | flops 524288 | bytes 1835008 | tf_op jit(solution)/shard_map/concatenate | solution.py:97
  87.0 5.1 %collective-permute-start.5 = (bf16[2,2,256,256]{3,2,1,0:T(8,128)(2,1)}, bf16[2,2,256,256]{3,2,1,0:T(8,128)(2,1)}, u32[]{:S(2)}, u32[]{:S(2)}) collective-permute-start(bf16[2,2,256,256]{3,2,1,0:T(8,128)(2,1)} %get-tuple-element.50), channel_id=1, source_target_pairs={{0,8},{4,12},{8,16},{12,20},{16,24},{20,28},{1,9},{5,13},{9,17},{1... | collective-permute-start | bytes 1572872 | tf_op jit(solution)/shard_map/ppermute | solution.py:16
  100.1 1.9 %collective-permute-start.8 = (bf16[2,2,256,256]{3,2,1,0:T(8,128)(2,1)S(1)}, bf16[2,2,256,256]{3,2,1,0:T(8,128)(2,1)}, u32[]{:S(2)}, u32[]{:S(2)}) collective-permute-start(bf16[2,2,256,256]{3,2,1,0:T(8,128)(2,1)S(1)} %get-tuple-element.49), channel_id=1, source_target_pairs={{8,0},{12,4},{16,8},{20,12},{24,16},{28,20},{9,1},{13,5},{17,9},{2... | collective-permute-start | bytes 1572872 | tf_op jit(solution)/shard_map/ppermute | solution.py:16
  104.3 2.4 %fusion.37 = f32[1,64,4,4,64]{1,4,3,2,0:T(8,128)} fusion(f32[4,4,64,192]{3,2,1,0:T(8,128)S(1)} %get-tuple-element.65, bf16[1,64,4,4,64]{1,4,3,2,0:T(8,128)(2,1)} %copy.136, bf16[1,64,4,4,64]{1,4,3,2,0:T(8,128)(2,1)} %copy.135, bf16[1,64,4,4,64]{1,4,3,2,0:T(8,128)(2,1)} %copy.134, f32[4,4,64]{2,1,0:T(4,128)S(1)} %get-tuple-element.64, f32[64,4,4]{0,2,1:T(4,128)} %bitcast.233), kind=kOutput, calls=%fused_computation.49 | convolution fusion | flops 26804224 | bytes 1449984 | tf_op jit(solution)/shard_map/brhqk,bkrhe->bqrhe/dot_general | solution.py:84
  111.1 2.9 %collective-permute-done.8 = bf16[2,2,256,256]{3,2,1,0:T(8,128)(2,1)} collective-permute-done((bf16[2,2,256,256]{3,2,1,0:T(8,128)(2,1)S(1)}, bf16[2,2,256,256]{3,2,1,0:T(8,128)(2,1)}, u32[]{:S(2)}, u32[]{:S(2)}) %collective-permute-start.8) | collective-permute-done | bytes 524320 | tf_op jit(solution)/shard_map/ppermute | solution.py:16
  129.0 9.6 %concatenate.99 = bf16[1,144,16,4,64]{1,4,3,2,0:T(8,128)(2,1)S(1)} concatenate(bf16[1,16,16,4,64]{1,4,3,2,0:T(8,128)(2,1)} %copy.116, bf16[1,16,16,4,64]{1,4,3,2,0:T(8,128)(2,1)} %copy.117, bf16[1,16,16,4,64]{1,4,3,2,0:T(8,128)(2,1)} %copy.118, bf16[1,16,16,4,64]{1,4,3,2,0:T(8,128)(2,1)} %copy.119, bf16[1,16,16,4,64]{1,4,3,2,0:T(8,128)(2,1)S(1)} %copy.120, ...), dimensions={1} | concatenate | bytes 2359296 | tf_op jit(solution)/shard_map/concatenate | solution.py:57
  148.5 2.5 %copy.143 = bf16[1,16,16,4,64]{1,4,3,2,0:T(8,128)(2,1)} copy(bf16[1,16,16,4,64]{4,3,2,1,0:T(4,128)(2,1)} %slice.368) | data formatting | bytes 262144 | tf_op jit(solution)/shard_map/slice | solution.py:61
  151.0 1.8 slice.370
  152.8 2.3 %copy.144 = bf16[1,16,16,4,64]{1,4,3,2,0:T(8,128)(2,1)} copy(bf16[1,16,16,4,64]{4,3,2,1,0:T(4,128)(2,1)} %slice.370) | data formatting | bytes 262144 | tf_op jit(solution)/shard_map/slice | solution.py:61
  155.1 1.8 slice.372
  156.9 2.4 %copy.145 = bf16[1,16,16,4,64]{1,4,3,2,0:T(8,128)(2,1)} copy(bf16[1,16,16,4,64]{4,3,2,1,0:T(4,128)(2,1)} %slice.372) | data formatting | bytes 262144 | tf_op jit(solution)/shard_map/slice | solution.py:61
  160.2 2.4 %copy.146 = bf16[1,16,16,4,64]{1,4,3,2,0:T(8,128)(2,1)} copy(bf16[1,16,16,4,64]{4,3,2,1,0:T(4,128)(2,1)} %slice.374) | data formatting | bytes 262144 | tf_op jit(solution)/shard_map/slice | solution.py:61
  162.6 10.3 %concatenate.102 = bf16[1,144,16,4,64]{1,4,3,2,0:T(8,128)(2,1)} concatenate(bf16[1,16,16,4,64]{1,4,3,2,0:T(8,128)(2,1)S(1)} %copy.138, bf16[1,16,16,4,64]{1,4,3,2,0:T(8,128)(2,1)} %copy.139, bf16[1,16,16,4,64]{1,4,3,2,0:T(8,128)(2,1)} %copy.140, bf16[1,16,16,4,64]{1,4,3,2,0:T(8,128)(2,1)} %copy.141, bf16[1,16,16,4,64]{1,4,3,2,0:T(8,128)(2,1)S(1)} %copy-done.3, ...), dimensions={1} | concatenate | bytes 2359296 | tf_op jit(solution)/shard_map/concatenate | solution.py:60
  172.9 2.4 %fusion.33 = f32[1,16,16,4,64]{4,1,3,2,0:T(8,128)S(1)} fusion(bf16[1,144,16,4,64]{1,4,3,2,0:T(8,128)(2,1)} %concatenate.102, f32[16,4,16,144]{3,2,1,0:T(8,128)S(1)} %get-tuple-element.63, f32[16,4,16]{2,1,0:T(4,128)S(1)} %copy-done.24, f32[16,16,4]{0,2,1:T(4,128)S(1)} %bitcast.232), kind=kOutput, calls=%fused_computation.47 | convolution fusion | flops 19234816 | bytes 2039808 | tf_op jit(solution)/shard_map/brhqk,bkrhe->bqrhe/dot_general | solution.py:84
  176.0 9.4 %all_gather.3 = bf16[256,1024]{0,1:T(8,128)(2,1)S(1)} all-gather(bf16[256,256]{0,1:T(8,128)(2,1)S(1)} %bitcast.228), channel_id=1, replica_groups=mesh['sp'=8,'tp'=4] {'tp'}, dimensions={1}, use_global_device_ids=true | all-gather | bytes 655360 | tf_op jit(solution)/shard_map/all_gather | solution.py:152
  (208 shorter events, 81.3 us)
Async XLA Ops:
  0.0 5.4 %copy-start = (bf16[256,2048]{1,0:T(8,128)(2,1)S(1)}, bf16[256,2048]{1,0:T(8,128)(2,1)}, u32[]{:S(2)}) copy-start(bf16[256,2048]{1,0:T(8,128)(2,1)} %param.5) | copy-start | bytes 3145732
  7.1 14.1 %copy-start.16 = (bf16[256,256]{1,0:T(8,128)(2,1)}, bf16[256,256]{1,0:T(8,128)(2,1)S(1)}, u32[]{:S(2)}) copy-start(bf16[256,256]{1,0:T(8,128)(2,1)S(1)} %convolution_convert_fusion.1) | copy-start | bytes 393220
  12.4 14.6 %copy-start.4 = (bf16[3,2048,256]{2,1,0:T(8,128)(2,1)S(1)}, bf16[3,2048,256]{2,1,0:T(8,128)(2,1)}, u32[]{:S(2)}) copy-start(bf16[3,2048,256]{2,1,0:T(8,128)(2,1)} %param.6) | copy-start | bytes 9437188
  14.2 94.7 %collective-permute-start.6 = (bf16[1,2,256,256]{3,2,1,0:T(8,128)(2,1)}, bf16[1,2,256,256]{3,2,1,0:T(8,128)(2,1)}, u32[]{:S(2)}, u32[]{:S(2)}) collective-permute-start(bf16[1,2,256,256]{3,2,1,0:T(8,128)(2,1)} %maximum_bitcast_fusion.9), channel_id=1, source_target_pairs={{0,16},{4,20},{8,24},{12,28},{1,17},{5,21},{9,25},{13,29},{2,18},{... | collective-permute-start | bytes 786440 | tf_op jit(solution)/shard_map/ppermute | solution.py:16
  19.1 61.9 %collective-permute-start.7 = (bf16[1,2,256,256]{3,2,1,0:T(8,128)(2,1)}, bf16[1,2,256,256]{3,2,1,0:T(8,128)(2,1)}, u32[]{:S(2)}, u32[]{:S(2)}) collective-permute-start(bf16[1,2,256,256]{3,2,1,0:T(8,128)(2,1)} %maximum_bitcast_fusion.9), channel_id=1, source_target_pairs={{4,0},{8,4},{12,8},{16,12},{20,16},{24,20},{28,24},{5,1},{9,5},{13... | collective-permute-start | bytes 786440 | tf_op jit(solution)/shard_map/ppermute | solution.py:16
  21.2 63.8 %collective-permute-start.4 = (bf16[1,2,256,256]{3,2,1,0:T(8,128)(2,1)}, bf16[1,2,256,256]{3,2,1,0:T(8,128)(2,1)}, u32[]{:S(2)}, u32[]{:S(2)}) collective-permute-start(bf16[1,2,256,256]{3,2,1,0:T(8,128)(2,1)} %maximum_bitcast_fusion.9), channel_id=1, source_target_pairs={{0,4},{4,8},{8,12},{12,16},{16,20},{20,24},{24,28},{1,5},{5,9},{9,... | collective-permute-start | bytes 786440 | tf_op jit(solution)/shard_map/ppermute | solution.py:16
  40.1 2.5 %copy-start.2 = (bf16[256,2048]{0,1:T(8,128)(2,1)S(1)}, bf16[256,2048]{0,1:T(8,128)(2,1)}, u32[]{:S(2)}) copy-start(bf16[256,2048]{0,1:T(8,128)(2,1)} %get-tuple-element.6) | copy-start | bytes 3145732
  47.6 8.3 %copy-start.17 = (bf16[256,256]{1,0:T(8,128)(2,1)S(1)}, bf16[256,256]{1,0:T(8,128)(2,1)}, u32[]{:S(2)}) copy-start(bf16[256,256]{1,0:T(8,128)(2,1)} %copy-done.16) | copy-start | bytes 393220
  50.6 19.9 %collective-permute-start = (bf16[2,64,256]{2,1,0:T(8,128)(2,1)}, bf16[2,64,256]{2,1,0:T(8,128)(2,1)}, u32[]{:S(2)}, u32[]{:S(2)}) collective-permute-start(bf16[2,64,256]{2,1,0:T(8,128)(2,1)} %get-tuple-element.35), channel_id=1, source_target_pairs={{0,4},{4,8},{8,12},{12,16},{16,20},{20,24},{24,28},{1,5},{5,9},{9,... | collective-permute-start | bytes 196616 | tf_op jit(solution)/shard_map/ppermute | solution.py:24
  52.5 19.4 %collective-permute-start.1 = (bf16[2,64,256]{2,1,0:T(8,128)(2,1)}, bf16[2,64,256]{2,1,0:T(8,128)(2,1)}, u32[]{:S(2)}, u32[]{:S(2)}) collective-permute-start(bf16[2,64,256]{2,1,0:T(8,128)(2,1)} %get-tuple-element.36), channel_id=1, source_target_pairs={{4,0},{8,4},{12,8},{16,12},{20,16},{24,20},{28,24},{5,1},{9,5},{13... | collective-permute-start | bytes 196616 | tf_op jit(solution)/shard_map/ppermute | solution.py:27
  56.2 5.1 %copy-start.20 = (bf16[256,4,64]{0,2,1:T(8,128)(2,1)S(1)}, bf16[256,4,64]{0,2,1:T(8,128)(2,1)}, u32[]{:S(2)}) copy-start(bf16[256,4,64]{0,2,1:T(8,128)(2,1)} %get-tuple-element.57) | copy-start | bytes 393220
  58.5 5.5 %copy-start.19 = (bf16[256,4,64]{0,2,1:T(8,128)(2,1)S(1)}, bf16[256,4,64]{0,2,1:T(8,128)(2,1)}, u32[]{:S(2)}) copy-start(bf16[256,4,64]{0,2,1:T(8,128)(2,1)} %get-tuple-element.55) | copy-start | bytes 393220
  59.3 6.7 %copy-start.18 = (bf16[256,4,64]{0,2,1:T(8,128)(2,1)S(1)}, bf16[256,4,64]{0,2,1:T(8,128)(2,1)}, u32[]{:S(2)}) copy-start(bf16[256,4,64]{0,2,1:T(8,128)(2,1)} %get-tuple-element.53) | copy-start | bytes 393220
  70.5 7.5 %copy-start.29 = (pred[4,64,192]{2,1,0:T(8,128)(4,1)S(1)}, pred[4,64,192]{2,1,0:T(8,128)(4,1)}, u32[]{:S(2)}) copy-start(pred[4,64,192]{2,1,0:T(8,128)(4,1)} %get-tuple-element.60) | copy-start | bytes 147460
  70.5 40.6 %collective-permute-start.9 = (bf16[1,2,256,256]{3,2,1,0:T(8,128)(2,1)}, bf16[1,2,256,256]{3,2,1,0:T(8,128)(2,1)}, u32[]{:S(2)}, u32[]{:S(2)}) collective-permute-start(bf16[1,2,256,256]{3,2,1,0:T(8,128)(2,1)} %maximum_bitcast_fusion.9), channel_id=1, source_target_pairs={{16,0},{20,4},{24,8},{28,12},{17,1},{21,5},{25,9},{29,13},{18,2},{... | collective-permute-start | bytes 786440 | tf_op jit(solution)/shard_map/ppermute | solution.py:16
  71.9 20.2 %collective-permute-start.3 = (bf16[2,256,256]{2,1,0:T(8,128)(2,1)}, bf16[2,256,256]{2,1,0:T(8,128)(2,1)}, u32[]{:S(2)}, u32[]{:S(2)}) collective-permute-start(bf16[2,256,256]{2,1,0:T(8,128)(2,1)} %pad_maximum_fusion.3), channel_id=1, source_target_pairs={{4,0},{8,4},{12,8},{16,12},{20,16},{24,20},{28,24},{5,1},{9,5},{13... | collective-permute-start | bytes 786440 | tf_op jit(solution)/shard_map/ppermute | solution.py:27
  81.0 15.0 %collective-permute-start.2 = (bf16[2,256,256]{2,1,0:T(8,128)(2,1)}, bf16[2,256,256]{2,1,0:T(8,128)(2,1)S(1)}, u32[]{:S(2)}, u32[]{:S(2)}) collective-permute-start(bf16[2,256,256]{2,1,0:T(8,128)(2,1)} %pad_maximum_fusion.3), channel_id=1, source_target_pairs={{0,4},{4,8},{8,12},{12,16},{16,20},{20,24},{24,28},{1,5},{5,9},{9,... | collective-permute-start | bytes 786440 | tf_op jit(solution)/shard_map/ppermute | solution.py:24
  87.0 21.9 %collective-permute-start.5 = (bf16[2,2,256,256]{3,2,1,0:T(8,128)(2,1)}, bf16[2,2,256,256]{3,2,1,0:T(8,128)(2,1)}, u32[]{:S(2)}, u32[]{:S(2)}) collective-permute-start(bf16[2,2,256,256]{3,2,1,0:T(8,128)(2,1)} %get-tuple-element.50), channel_id=1, source_target_pairs={{0,8},{4,12},{8,16},{12,20},{16,24},{20,28},{1,9},{5,13},{9,17},{1... | collective-permute-start | bytes 1572872 | tf_op jit(solution)/shard_map/ppermute | solution.py:16
  99.1 2.9 %copy-start.30 = (f32[4,4,64]{2,1,0:T(4,128)}, f32[4,4,64]{2,1,0:T(4,128)S(1)}, u32[]{:S(2)}) copy-start(f32[4,4,64]{2,1,0:T(4,128)S(1)} %fusion.41) | copy-start | bytes 12292
  100.1 13.9 %collective-permute-start.8 = (bf16[2,2,256,256]{3,2,1,0:T(8,128)(2,1)S(1)}, bf16[2,2,256,256]{3,2,1,0:T(8,128)(2,1)}, u32[]{:S(2)}, u32[]{:S(2)}) collective-permute-start(bf16[2,2,256,256]{3,2,1,0:T(8,128)(2,1)S(1)} %get-tuple-element.49), channel_id=1, source_target_pairs={{8,0},{12,4},{16,8},{20,12},{24,16},{28,20},{9,1},{13,5},{17,9},{2... | collective-permute-start | bytes 1572872 | tf_op jit(solution)/shard_map/ppermute | solution.py:16
  140.1 2.8 %copy-start.13 = (bf16[1,256,256]{2,1,0:T(8,128)(2,1)S(1)}, bf16[1,256,256]{2,1,0:T(8,128)(2,1)}, u32[]{:S(2)}) copy-start(bf16[1,256,256]{2,1,0:T(8,128)(2,1)} %get-tuple-element.22) | copy-start | bytes 393220
  140.1 4.4 %copy-start.12 = (bf16[1,256,256]{2,1,0:T(8,128)(2,1)S(1)}, bf16[1,256,256]{2,1,0:T(8,128)(2,1)}, u32[]{:S(2)}) copy-start(bf16[1,256,256]{2,1,0:T(8,128)(2,1)} %get-tuple-element.21) | copy-start | bytes 393220
  142.3 5.3 %copy-start.15 = (bf16[1,256,256]{2,1,0:T(8,128)(2,1)S(1)}, bf16[1,256,256]{2,1,0:T(8,128)(2,1)}, u32[]{:S(2)}) copy-start(bf16[1,256,256]{2,1,0:T(8,128)(2,1)} %get-tuple-element.15) | copy-start | bytes 393220
  146.2 13.1 %copy-start.14 = (bf16[1,256,256]{2,1,0:T(8,128)(2,1)S(1)}, bf16[1,256,256]{2,1,0:T(8,128)(2,1)}, u32[]{:S(2)}) copy-start(bf16[1,256,256]{2,1,0:T(8,128)(2,1)} %get-tuple-element.12) | copy-start | bytes 393220
  148.5 14.0 %copy-start.3 = (bf16[1,16,16,4,64]{1,4,3,2,0:T(8,128)(2,1)S(1)}, bf16[1,16,16,4,64]{1,4,3,2,0:T(8,128)(2,1)}, u32[]{:S(2)}) copy-start(bf16[1,16,16,4,64]{1,4,3,2,0:T(8,128)(2,1)} %copy.142) | copy-start | bytes 393220
  162.6 10.3 %copy-start.24 = (f32[16,4,16]{2,1,0:T(4,128)S(1)}, f32[16,4,16]{2,1,0:T(4,128)}, u32[]{:S(2)}) copy-start(f32[16,4,16]{2,1,0:T(4,128)} %copy-done.23) | copy-start | bytes 12292
  162.6 10.3 %copy-start.28 = (f32[16,4,16]{2,1,0:T(4,128)S(1)}, f32[16,4,16]{2,1,0:T(4,128)}, u32[]{:S(2)}) copy-start(f32[16,4,16]{2,1,0:T(4,128)} %copy-done.27) | copy-start | bytes 12292
  172.9 3.0 %copy-start.31 = (f32[256,4]{0,1:T(4,128)S(1)}, f32[256,4]{0,1:T(4,128)}, u32[]{:S(2)}) copy-start(f32[256,4]{0,1:T(4,128)} %stack_reshape.12) | copy-start | bytes 12292
  172.9 3.0 %copy-start.32 = (f32[256,4]{0,1:T(4,128)S(1)}, f32[256,4]{0,1:T(4,128)}, u32[]{:S(2)}) copy-start(f32[256,4]{0,1:T(4,128)} %stack_reshape.13) | copy-start | bytes 12292
  172.9 3.0 %copy-start.5 = (f32[1,256,4,64]{1,3,2,0:T(8,128)S(1)}, f32[1,256,4,64]{1,3,2,0:T(8,128)}, u32[]{:S(2)}) copy-start(f32[1,256,4,64]{1,3,2,0:T(8,128)} %copy.148) | copy-start | bytes 786436
  172.9 13.7 %copy-start.1 = (bf16[256,2048]{1,0:T(8,128)(2,1)S(1)}, bf16[256,2048]{1,0:T(8,128)(2,1)}, u32[]{:S(2)}) copy-start(bf16[256,2048]{1,0:T(8,128)(2,1)} %param.5) | copy-start | bytes 3145732
  175.3 10.1 %copy-start.33 = (bf16[1024,512]{1,0:T(8,128)(2,1)S(1)}, bf16[1024,512]{1,0:T(8,128)(2,1)}, u32[]{:S(2)}) copy-start(bf16[1024,512]{1,0:T(8,128)(2,1)} %param.9) | copy-start | bytes 3145732
  (12 other events, 16.2 us)
where the time goes:
time: 189 us; the launch traced here: 187 us
  local copies, waits for them, and re-layouts  93.4 us (49%)
  starting transfers between devices  31.2 us (17%)
  matrix products  26.3 us (14%)
  other arithmetic  20.8 us (11%)
  blocking collectives  9.43 us (5%)
  waiting for transfers between devices  4.54 us (2%)
    slice x32, local copies, waits for them, and re-layouts, banded(): value_blocks[shift_idx:shift_idx + blocks]  29.6 us
    ppermute x6, starting transfers between devices, shifted(): return lax.ppermute(block, axis, route)  19.6 us
    slice x26, local copies, waits for them, and re-layouts, banded(): key_blocks[shift_idx:shift_idx + blocks]  17.3 us
    concatenate x1, local copies, waits for them, and re-layouts, banded(): jnp.concatenate([value_blocks[shift_idx:shift_idx + blocks] for shift_idx...  10.3 us
    concatenate x1, local copies, waits for them, and re-layouts, banded(): jnp.concatenate([key_blocks[shift_idx:shift_idx + blocks] for shift_idx i...  9.59 us
    all_gather x1, blocking collectives, per_device(): lax.all_gather(merged, 'tp', axis=1, tiled=True)  9.43 us
    dot_general x4, local copies, waits for them, and re-layouts, per_device(): jnp.dot(tokens, query_weight[group_idx], preferred_element_type=jnp.float32)  7.65 us
    dot_general x4, local copies, waits for them, and re-layouts, per_device(): jnp.dot(tokens, key_weight[group_idx], preferred_element_type=jnp.float32)  7.46 us
  transfers between devices with their start and end apart: 10, of which 2 were waited for; matrix products, arithmetic and copies ran while one was open for 34% of the time, Pallas kernels for 0%

commit v1 on v0

--- a/solution.py
+++ b/solution.py
@@ -149,7 +149,7 @@
         jnp.sum(merge_w[..., None] * stacked, axis=0).reshape(length, columns).astype(jnp.bfloat16)
     )
     mixed = jnp.dot(
-        lax.all_gather(merged, "tp", axis=1, tiled=True),
+        jnp.concatenate(lax.all_gather(merged, "tp"), axis=1),
         out_weight,
         preferred_element_type=jnp.float32,
     )

time: 189 us -> 183 us (0.968)
  other arithmetic: 20.8 us -> 12.8 us
  waiting for transfers between devices: 4.54 us -> 8.34 us
    ppermute x6, waiting for transfers between devices: 2.91 us -> 5.44 us  [shifted(): return lax.ppermute(block, axis, route)]
    and x4, other arithmetic: 3.86 us -> 1.36 us  [banded(): within[None, None, None]]
    slice x32, local copies, waits for them, and re-layouts: 29.6 us -> 27.3 us  [banded(): value_blocks[shift_idx:shift_idx + blocks]]
  transfers between devices with their start and end apart: 10 -> 10, of which waited for: 2 -> 2; matrix products, arithmetic and copies ran while one was open for 34% -> 29% of each run, Pallas kernels for 0% -> 0%
where the time goes in v1:
time: 183 us; the launch traced here: 181 us
  local copies, waits for them, and re-layouts  92.4 us (50%)
  starting transfers between devices  30.5 us (17%)
  matrix products  26.4 us (14%)
  other arithmetic  12.8 us (7%)
  blocking collectives  9.51 us (5%)
  waiting for transfers between devices  8.34 us (5%)
    slice x32, local copies, waits for them, and re-layouts, banded(): value_blocks[shift_idx:shift_idx + blocks]  27.3 us
    ppermute x6, starting transfers between devices, shifted(): return lax.ppermute(block, axis, route)  18.8 us
    slice x26, local copies, waits for them, and re-layouts, banded(): key_blocks[shift_idx:shift_idx + blocks]  18 us
    concatenate x1, local copies, waits for them, and re-layouts, banded(): jnp.concatenate([value_blocks[shift_idx:shift_idx + blocks] for shift_idx...  10.3 us
    concatenate x1, local copies, waits for them, and re-layouts, banded(): jnp.concatenate([key_blocks[shift_idx:shift_idx + blocks] for shift_idx i...  9.81 us
    all_gather x1, blocking collectives, per_device(): lax.all_gather(merged, 'tp')  9.51 us
    dot_general x4, local copies, waits for them, and re-layouts, per_device(): jnp.dot(tokens, query_weight[group_idx], preferred_element_type=jnp.float32)  7.66 us
    dot_general x4, local copies, waits for them, and re-layouts, per_device(): jnp.dot(tokens, key_weight[group_idx], preferred_element_type=jnp.float32)  7.44 us
  transfers between devices with their start and end apart: 10, of which 2 were waited for; matrix products, arithmetic and copies ran while one was open for 29% of the time, Pallas kernels for 0%

profile of v1, /device:TPU:13, one launch (start us, length us, event | category | flops | bytes accessed | tf_op | source)
XLA Modules:
  0.0 181.0 jit_solution(16872456832766705336)
XLA Ops:
  0.0 3.1 %slice_bitcast_fusion.4 = (bf16[256,2048]{0,1:T(8,128)(2,1)S(1)}, bf16[256,2048]{0,1:T(8,128)(2,1)}, bf16[256,2048]{0,1:T(8,128)(2,1)S(1)}) fusion(bf16[3,2048,256]{2,1,0:T(8,128)(2,1)} %param.7), kind=kLoop, calls=%fused_computation.45 | loop fusion | bytes 6291456 | tf_op jit(solution)/shard_map/dot_general | solution.py:113
  3.1 2.3 %copy.111 = bf16[256,2048]{1,0:T(8,128)(2,1)} copy(bf16[256,2048]{0,1:T(8,128)(2,1)} %get-tuple-element.9) | data formatting | bytes 2097152 | tf_op jit(solution)/shard_map/dot_general | solution.py:113
  7.1 1.7 fusion.18
  12.4 1.8 maximum_bitcast_fusion.9
  14.1 4.9 %collective-permute-start.6 = (bf16[1,2,256,256]{3,2,1,0:T(8,128)(2,1)}, bf16[1,2,256,256]{3,2,1,0:T(8,128)(2,1)}, u32[]{:S(2)}, u32[]{:S(2)}) collective-permute-start(bf16[1,2,256,256]{3,2,1,0:T(8,128)(2,1)} %maximum_bitcast_fusion.9), channel_id=1, source_target_pairs={{0,16},{4,20},{8,24},{12,28},{1,17},{5,21},{9,25},{13,29},{2,18},{... | collective-permute-start | bytes 786440 | tf_op jit(solution)/shard_map/ppermute | solution.py:16
  19.1 2.1 %collective-permute-start.7 = (bf16[1,2,256,256]{3,2,1,0:T(8,128)(2,1)}, bf16[1,2,256,256]{3,2,1,0:T(8,128)(2,1)}, u32[]{:S(2)}, u32[]{:S(2)}) collective-permute-start(bf16[1,2,256,256]{3,2,1,0:T(8,128)(2,1)} %maximum_bitcast_fusion.9), channel_id=1, source_target_pairs={{4,0},{8,4},{12,8},{16,12},{20,16},{24,20},{28,24},{5,1},{9,5},{13... | collective-permute-start | bytes 786440 | tf_op jit(solution)/shard_map/ppermute | solution.py:16
  21.2 4.0 %collective-permute-start.4 = (bf16[1,2,256,256]{3,2,1,0:T(8,128)(2,1)}, bf16[1,2,256,256]{3,2,1,0:T(8,128)(2,1)}, u32[]{:S(2)}, u32[]{:S(2)}) collective-permute-start(bf16[1,2,256,256]{3,2,1,0:T(8,128)(2,1)} %maximum_bitcast_fusion.9), channel_id=1, source_target_pairs={{0,4},{4,8},{8,12},{12,16},{16,20},{20,24},{24,28},{1,5},{5,9},{9,... | collective-permute-start | bytes 786440 | tf_op jit(solution)/shard_map/ppermute | solution.py:16
  26.9 1.7 slice_bitcast_fusion.5
  28.6 2.3 %copy.91 = bf16[256,2048]{1,0:T(8,128)(2,1)} copy(bf16[256,2048]{0,1:T(8,128)(2,1)} %get-tuple-element.5) | data formatting | bytes 2097152 | tf_op jit(solution)/shard_map/dot_general | solution.py:110
  30.9 1.7 fusion.28
  34.0 2.3 %copy.99 = bf16[256,2048]{1,0:T(8,128)(2,1)} copy(bf16[256,2048]{0,1:T(8,128)(2,1)} %get-tuple-element.7) | data formatting | bytes 2097152 | tf_op jit(solution)/shard_map/dot_general | solution.py:110
  36.3 2.4 %fusion.24 = f32[256,4,64]{0,2,1:T(8,128)} fusion(bf16[4,64,2048]{2,1,0:T(8,128)(2,1)} %bitcast.225, bf16[256,2048]{1,0:T(8,128)(2,1)S(1)} %copy-done), kind=kOutput, calls=%fused_computation.28 | convolution fusion | flops 268435456 | bytes 2359296 | tf_op jit(solution)/shard_map/dot_general | solution.py:110
  40.1 2.5 %fusion.26 = f32[256,4,64]{0,2,1:T(8,128)} fusion(bf16[4,64,2048]{2,1,0:T(8,128)(2,1)} %bitcast.226, bf16[256,2048]{1,0:T(8,128)(2,1)S(1)} %copy-done), kind=kOutput, calls=%fused_computation.30 | convolution fusion | flops 268435456 | bytes 2359296 | tf_op jit(solution)/shard_map/dot_general | solution.py:113
  44.0 2.4 %fusion.20 = f32[256,4,64]{0,2,1:T(8,128)} fusion(bf16[4,64,2048]{2,1,0:T(8,128)(2,1)} %bitcast.227, bf16[256,2048]{1,0:T(8,128)(2,1)S(1)} %copy-done), kind=kOutput, calls=%fused_computation.24 | convolution fusion | flops 268435456 | bytes 2359296 | tf_op jit(solution)/shard_map/dot_general | solution.py:110
  49.3 1.9 %collective-permute-start = (bf16[2,64,256]{2,1,0:T(8,128)(2,1)S(1)}, bf16[2,64,256]{2,1,0:T(8,128)(2,1)S(1)}, u32[]{:S(2)}, u32[]{:S(2)}) collective-permute-start(bf16[2,64,256]{2,1,0:T(8,128)(2,1)S(1)} %get-tuple-element.35), channel_id=1, source_target_pairs={{0,4},{4,8},{8,12},{12,16},{16,20},{20,24},{24,28},{1,5},{5,9},{9,... | collective-permute-start | bytes 196616 | tf_op jit(solution)/shard_map/ppermute | solution.py:24
  51.2 3.4 %collective-permute-start.1 = (bf16[2,64,256]{2,1,0:T(8,128)(2,1)S(1)}, bf16[2,64,256]{2,1,0:T(8,128)(2,1)S(1)}, u32[]{:S(2)}, u32[]{:S(2)}) collective-permute-start(bf16[2,64,256]{2,1,0:T(8,128)(2,1)S(1)} %get-tuple-element.36), channel_id=1, source_target_pairs={{4,0},{8,4},{12,8},{16,12},{20,16},{24,20},{28,24},{5,1},{9,5},{13... | collective-permute-start | bytes 196616 | tf_op jit(solution)/shard_map/ppermute | solution.py:27
  66.4 2.3 %collective-permute-start.3 = (bf16[2,256,256]{2,1,0:T(8,128)(2,1)S(1)}, bf16[2,256,256]{2,1,0:T(8,128)(2,1)S(1)}, u32[]{:S(2)}, u32[]{:S(2)}) collective-permute-start(bf16[2,256,256]{2,1,0:T(8,128)(2,1)S(1)} %pad_maximum_fusion.3), channel_id=1, source_target_pairs={{4,0},{8,4},{12,8},{16,12},{20,16},{24,20},{28,24},{5,1},{9,5},{13... | collective-permute-start | bytes 786440 | tf_op jit(solution)/shard_map/ppermute | solution.py:27
  75.0 4.0 %collective-permute-start.2 = (bf16[2,256,256]{2,1,0:T(8,128)(2,1)S(1)}, bf16[2,256,256]{2,1,0:T(8,128)(2,1)S(1)}, u32[]{:S(2)}, u32[]{:S(2)}) collective-permute-start(bf16[2,256,256]{2,1,0:T(8,128)(2,1)S(1)} %pad_maximum_fusion.3), channel_id=1, source_target_pairs={{0,4},{4,8},{8,12},{12,16},{16,20},{20,24},{24,28},{1,5},{5,9},{9,... | collective-permute-start | bytes 786440 | tf_op jit(solution)/shard_map/ppermute | solution.py:24
  80.2 4.6 %collective-permute-start.5 = (bf16[2,2,256,256]{3,2,1,0:T(8,128)(2,1)S(1)}, bf16[2,2,256,256]{3,2,1,0:T(8,128)(2,1)}, u32[]{:S(2)}, u32[]{:S(2)}) collective-permute-start(bf16[2,2,256,256]{3,2,1,0:T(8,128)(2,1)S(1)} %get-tuple-element.50), channel_id=1, source_target_pairs={{0,8},{4,12},{8,16},{12,20},{16,24},{20,28},{1,9},{5,13},{9,17},{1... | collective-permute-start | bytes 1572872 | tf_op jit(solution)/shard_map/ppermute | solution.py:16
  86.0 2.9 %collective-permute-done.2 = bf16[2,256,256]{2,1,0:T(8,128)(2,1)S(1)} collective-permute-done((bf16[2,256,256]{2,1,0:T(8,128)(2,1)S(1)}, bf16[2,256,256]{2,1,0:T(8,128)(2,1)S(1)}, u32[]{:S(2)}, u32[]{:S(2)}) %collective-permute-start.2) | collective-permute-done | bytes 262176 | tf_op jit(solution)/shard_map/ppermute | solution.py:24
  93.0 1.9 %collective-permute-start.8 = (bf16[2,2,256,256]{3,2,1,0:T(8,128)(2,1)S(1)}, bf16[2,2,256,256]{3,2,1,0:T(8,128)(2,1)}, u32[]{:S(2)}, u32[]{:S(2)}) collective-permute-start(bf16[2,2,256,256]{3,2,1,0:T(8,128)(2,1)S(1)} %get-tuple-element.49), channel_id=1, source_target_pairs={{8,0},{12,4},{16,8},{20,12},{24,16},{28,20},{9,1},{13,5},{17,9},{2... | collective-permute-start | bytes 1572872 | tf_op jit(solution)/shard_map/ppermute | solution.py:16
  101.4 5.4 %collective-permute-done.8 = bf16[2,2,256,256]{3,2,1,0:T(8,128)(2,1)} collective-permute-done((bf16[2,2,256,256]{3,2,1,0:T(8,128)(2,1)S(1)}, bf16[2,2,256,256]{3,2,1,0:T(8,128)(2,1)}, u32[]{:S(2)}, u32[]{:S(2)}) %collective-permute-start.8) | collective-permute-done | bytes 524320 | tf_op jit(solution)/shard_map/ppermute | solution.py:16
  121.9 9.8 %concatenate.99 = bf16[1,144,16,4,64]{1,4,3,2,0:T(8,128)(2,1)S(1)} concatenate(bf16[1,16,16,4,64]{1,4,3,2,0:T(8,128)(2,1)} %copy.116, bf16[1,16,16,4,64]{1,4,3,2,0:T(8,128)(2,1)} %copy.117, bf16[1,16,16,4,64]{1,4,3,2,0:T(8,128)(2,1)} %copy.118, bf16[1,16,16,4,64]{1,4,3,2,0:T(8,128)(2,1)} %copy.119, bf16[1,16,16,4,64]{1,4,3,2,0:T(8,128)(2,1)S(1)} %copy-done.4, ...), dimensions={1} | concatenate | bytes 2359296 | tf_op jit(solution)/shard_map/concatenate | solution.py:57
  142.5 2.4 %copy.143 = bf16[1,16,16,4,64]{1,4,3,2,0:T(8,128)(2,1)} copy(bf16[1,16,16,4,64]{4,3,2,1,0:T(4,128)(2,1)} %slice.368) | data formatting | bytes 262144 | tf_op jit(solution)/shard_map/slice | solution.py:61
  145.0 1.8 slice.370
  146.8 2.3 %copy.144 = bf16[1,16,16,4,64]{1,4,3,2,0:T(8,128)(2,1)} copy(bf16[1,16,16,4,64]{4,3,2,1,0:T(4,128)(2,1)} %slice.370) | data formatting | bytes 262144 | tf_op jit(solution)/shard_map/slice | solution.py:61
  149.1 1.8 slice.372
  150.9 2.4 %copy.145 = bf16[1,16,16,4,64]{1,4,3,2,0:T(8,128)(2,1)} copy(bf16[1,16,16,4,64]{4,3,2,1,0:T(4,128)(2,1)} %slice.372) | data formatting | bytes 262144 | tf_op jit(solution)/shard_map/slice | solution.py:61
  154.2 2.4 %copy.146 = bf16[1,16,16,4,64]{1,4,3,2,0:T(8,128)(2,1)} copy(bf16[1,16,16,4,64]{4,3,2,1,0:T(4,128)(2,1)} %slice.374) | data formatting | bytes 262144 | tf_op jit(solution)/shard_map/slice | solution.py:61
  156.6 10.3 %concatenate.102 = bf16[1,144,16,4,64]{1,4,3,2,0:T(8,128)(2,1)} concatenate(bf16[1,16,16,4,64]{1,4,3,2,0:T(8,128)(2,1)S(1)} %copy.138, bf16[1,16,16,4,64]{1,4,3,2,0:T(8,128)(2,1)} %copy.139, bf16[1,16,16,4,64]{1,4,3,2,0:T(8,128)(2,1)} %copy.140, bf16[1,16,16,4,64]{1,4,3,2,0:T(8,128)(2,1)} %copy.141, bf16[1,16,16,4,64]{1,4,3,2,0:T(8,128)(2,1)S(1)} %copy-done.3, ...), dimensions={1} | concatenate | bytes 2359296 | tf_op jit(solution)/shard_map/concatenate | solution.py:60
  166.9 2.3 %fusion.33 = f32[1,16,16,4,64]{4,1,3,2,0:T(8,128)S(1)} fusion(bf16[1,144,16,4,64]{1,4,3,2,0:T(8,128)(2,1)} %concatenate.102, f32[16,4,16,144]{3,2,1,0:T(8,128)S(1)} %get-tuple-element.63, f32[16,4,16]{2,1,0:T(4,128)S(1)} %copy-done.22, f32[16,16,4]{0,2,1:T(4,128)S(1)} %bitcast.236), kind=kOutput, calls=%fused_computation.47 | convolution fusion | flops 19234816 | bytes 2039808 | tf_op jit(solution)/shard_map/brhqk,bkrhe->bqrhe/dot_general | solution.py:84
  170.1 9.5 %all_gather.4 = bf16[4,256,256]{2,1,0:T(8,128)(2,1)S(1)} all-gather(bf16[1,256,256]{2,1,0:T(8,128)(2,1)S(1)} %copy.150), channel_id=1, replica_groups=mesh['sp'=8,'tp'=4] {'tp'}, dimensions={0}, use_global_device_ids=true | all-gather | bytes 655360 | tf_op jit(solution)/shard_map/all_gather | solution.py:152
  (202 shorter events, 73.2 us)
Async XLA Ops:
  0.0 5.4 %copy-start = (bf16[256,2048]{1,0:T(8,128)(2,1)S(1)}, bf16[256,2048]{1,0:T(8,128)(2,1)}, u32[]{:S(2)}) copy-start(bf16[256,2048]{1,0:T(8,128)(2,1)} %param.5) | copy-start | bytes 3145732
  7.1 14.1 %copy-start.17 = (bf16[256,256]{1,0:T(8,128)(2,1)}, bf16[256,256]{1,0:T(8,128)(2,1)S(1)}, u32[]{:S(2)}) copy-start(bf16[256,256]{1,0:T(8,128)(2,1)S(1)} %convolution_convert_fusion.1) | copy-start | bytes 393220
  12.4 14.6 %copy-start.5 = (bf16[3,2048,256]{2,1,0:T(8,128)(2,1)S(1)}, bf16[3,2048,256]{2,1,0:T(8,128)(2,1)}, u32[]{:S(2)}) copy-start(bf16[3,2048,256]{2,1,0:T(8,128)(2,1)} %param.6) | copy-start | bytes 9437188
  14.1 85.0 %collective-permute-start.6 = (bf16[1,2,256,256]{3,2,1,0:T(8,128)(2,1)}, bf16[1,2,256,256]{3,2,1,0:T(8,128)(2,1)}, u32[]{:S(2)}, u32[]{:S(2)}) collective-permute-start(bf16[1,2,256,256]{3,2,1,0:T(8,128)(2,1)} %maximum_bitcast_fusion.9), channel_id=1, source_target_pairs={{0,16},{4,20},{8,24},{12,28},{1,17},{5,21},{9,25},{13,29},{2,18},{... | collective-permute-start | bytes 786440 | tf_op jit(solution)/shard_map/ppermute | solution.py:16
  19.1 55.9 %collective-permute-start.7 = (bf16[1,2,256,256]{3,2,1,0:T(8,128)(2,1)}, bf16[1,2,256,256]{3,2,1,0:T(8,128)(2,1)}, u32[]{:S(2)}, u32[]{:S(2)}) collective-permute-start(bf16[1,2,256,256]{3,2,1,0:T(8,128)(2,1)} %maximum_bitcast_fusion.9), channel_id=1, source_target_pairs={{4,0},{8,4},{12,8},{16,12},{20,16},{24,20},{28,24},{5,1},{9,5},{13... | collective-permute-start | bytes 786440 | tf_op jit(solution)/shard_map/ppermute | solution.py:16
  21.2 57.8 %collective-permute-start.4 = (bf16[1,2,256,256]{3,2,1,0:T(8,128)(2,1)}, bf16[1,2,256,256]{3,2,1,0:T(8,128)(2,1)}, u32[]{:S(2)}, u32[]{:S(2)}) collective-permute-start(bf16[1,2,256,256]{3,2,1,0:T(8,128)(2,1)} %maximum_bitcast_fusion.9), channel_id=1, source_target_pairs={{0,4},{4,8},{8,12},{12,16},{16,20},{20,24},{24,28},{1,5},{5,9},{9,... | collective-permute-start | bytes 786440 | tf_op jit(solution)/shard_map/ppermute | solution.py:16
  40.1 2.5 %copy-start.2 = (bf16[256,2048]{0,1:T(8,128)(2,1)S(1)}, bf16[256,2048]{0,1:T(8,128)(2,1)}, u32[]{:S(2)}) copy-start(bf16[256,2048]{0,1:T(8,128)(2,1)} %get-tuple-element.6) | copy-start | bytes 3145732
  47.1 1.8 copy-start.9
  47.1 1.8 copy-start.10
  47.6 7.0 %copy-start.18 = (bf16[256,256]{1,0:T(8,128)(2,1)S(1)}, bf16[256,256]{1,0:T(8,128)(2,1)}, u32[]{:S(2)}) copy-start(bf16[256,256]{1,0:T(8,128)(2,1)} %copy-done.17) | copy-start | bytes 393220
  49.3 15.8 %collective-permute-start = (bf16[2,64,256]{2,1,0:T(8,128)(2,1)S(1)}, bf16[2,64,256]{2,1,0:T(8,128)(2,1)S(1)}, u32[]{:S(2)}, u32[]{:S(2)}) collective-permute-start(bf16[2,64,256]{2,1,0:T(8,128)(2,1)S(1)} %get-tuple-element.35), channel_id=1, source_target_pairs={{0,4},{4,8},{8,12},{12,16},{16,20},{20,24},{24,28},{1,5},{5,9},{9,... | collective-permute-start | bytes 196616 | tf_op jit(solution)/shard_map/ppermute | solution.py:24
  51.2 15.1 %collective-permute-start.1 = (bf16[2,64,256]{2,1,0:T(8,128)(2,1)S(1)}, bf16[2,64,256]{2,1,0:T(8,128)(2,1)S(1)}, u32[]{:S(2)}, u32[]{:S(2)}) collective-permute-start(bf16[2,64,256]{2,1,0:T(8,128)(2,1)S(1)} %get-tuple-element.36), channel_id=1, source_target_pairs={{4,0},{8,4},{12,8},{16,12},{20,16},{24,20},{28,24},{5,1},{9,5},{13... | collective-permute-start | bytes 196616 | tf_op jit(solution)/shard_map/ppermute | solution.py:27
  65.1 36.4 %collective-permute-start.9 = (bf16[1,2,256,256]{3,2,1,0:T(8,128)(2,1)}, bf16[1,2,256,256]{3,2,1,0:T(8,128)(2,1)}, u32[]{:S(2)}, u32[]{:S(2)}) collective-permute-start(bf16[1,2,256,256]{3,2,1,0:T(8,128)(2,1)} %maximum_bitcast_fusion.9), channel_id=1, source_target_pairs={{16,0},{20,4},{24,8},{28,12},{17,1},{21,5},{25,9},{29,13},{18,2},{... | collective-permute-start | bytes 786440 | tf_op jit(solution)/shard_map/ppermute | solution.py:16
  66.4 18.4 %collective-permute-start.3 = (bf16[2,256,256]{2,1,0:T(8,128)(2,1)S(1)}, bf16[2,256,256]{2,1,0:T(8,128)(2,1)S(1)}, u32[]{:S(2)}, u32[]{:S(2)}) collective-permute-start(bf16[2,256,256]{2,1,0:T(8,128)(2,1)S(1)} %pad_maximum_fusion.3), channel_id=1, source_target_pairs={{4,0},{8,4},{12,8},{16,12},{20,16},{24,20},{28,24},{5,1},{9,5},{13... | collective-permute-start | bytes 786440 | tf_op jit(solution)/shard_map/ppermute | solution.py:27
  71.6 2.0 %copy-start.23 = (bf16[4,64,1,4,64]{1,4,3,0,2:T(8,128)(2,1)S(1)}, bf16[4,64,1,4,64]{1,4,3,0,2:T(8,128)(2,1)}, u32[]{:S(2)}) copy-start(bf16[4,64,1,4,64]{1,4,3,0,2:T(8,128)(2,1)} %copy.130) | copy-start | bytes 393220
  74.3 15.7 %copy-start.26 = (pred[4,64,192]{2,1,0:T(8,128)(4,1)S(1)}, pred[4,64,192]{2,1,0:T(8,128)(4,1)}, u32[]{:S(2)}) copy-start(pred[4,64,192]{2,1,0:T(8,128)(4,1)} %get-tuple-element.61) | copy-start | bytes 147460
  75.0 13.9 %collective-permute-start.2 = (bf16[2,256,256]{2,1,0:T(8,128)(2,1)S(1)}, bf16[2,256,256]{2,1,0:T(8,128)(2,1)S(1)}, u32[]{:S(2)}, u32[]{:S(2)}) collective-permute-start(bf16[2,256,256]{2,1,0:T(8,128)(2,1)S(1)} %pad_maximum_fusion.3), channel_id=1, source_target_pairs={{0,4},{4,8},{8,12},{12,16},{16,20},{20,24},{24,28},{1,5},{5,9},{9,... | collective-permute-start | bytes 786440 | tf_op jit(solution)/shard_map/ppermute | solution.py:24
  80.2 19.0 %collective-permute-start.5 = (bf16[2,2,256,256]{3,2,1,0:T(8,128)(2,1)S(1)}, bf16[2,2,256,256]{3,2,1,0:T(8,128)(2,1)}, u32[]{:S(2)}, u32[]{:S(2)}) collective-permute-start(bf16[2,2,256,256]{3,2,1,0:T(8,128)(2,1)S(1)} %get-tuple-element.50), channel_id=1, source_target_pairs={{0,8},{4,12},{8,16},{12,20},{16,24},{20,28},{1,9},{5,13},{9,17},{1... | collective-permute-start | bytes 1572872 | tf_op jit(solution)/shard_map/ppermute | solution.py:16
  93.0 13.8 %collective-permute-start.8 = (bf16[2,2,256,256]{3,2,1,0:T(8,128)(2,1)S(1)}, bf16[2,2,256,256]{3,2,1,0:T(8,128)(2,1)}, u32[]{:S(2)}, u32[]{:S(2)}) collective-permute-start(bf16[2,2,256,256]{3,2,1,0:T(8,128)(2,1)S(1)} %get-tuple-element.49), channel_id=1, source_target_pairs={{8,0},{12,4},{16,8},{20,12},{24,16},{28,20},{9,1},{13,5},{17,9},{2... | collective-permute-start | bytes 1572872 | tf_op jit(solution)/shard_map/ppermute | solution.py:16
  115.6 6.3 %copy-start.4 = (bf16[1,16,16,4,64]{1,4,3,2,0:T(8,128)(2,1)S(1)}, bf16[1,16,16,4,64]{1,4,3,2,0:T(8,128)(2,1)}, u32[]{:S(2)}) copy-start(bf16[1,16,16,4,64]{1,4,3,2,0:T(8,128)(2,1)} %copy.120) | copy-start | bytes 393220
  133.2 3.7 %copy-start.14 = (bf16[1,256,256]{2,1,0:T(8,128)(2,1)S(1)}, bf16[1,256,256]{2,1,0:T(8,128)(2,1)}, u32[]{:S(2)}) copy-start(bf16[1,256,256]{2,1,0:T(8,128)(2,1)} %get-tuple-element.22) | copy-start | bytes 393220
  133.2 5.3 %copy-start.13 = (bf16[1,256,256]{2,1,0:T(8,128)(2,1)S(1)}, bf16[1,256,256]{2,1,0:T(8,128)(2,1)}, u32[]{:S(2)}) copy-start(bf16[1,256,256]{2,1,0:T(8,128)(2,1)} %get-tuple-element.21) | copy-start | bytes 393220
  136.3 5.3 %copy-start.16 = (bf16[1,256,256]{2,1,0:T(8,128)(2,1)S(1)}, bf16[1,256,256]{2,1,0:T(8,128)(2,1)}, u32[]{:S(2)}) copy-start(bf16[1,256,256]{2,1,0:T(8,128)(2,1)} %get-tuple-element.15) | copy-start | bytes 393220
  140.2 13.1 %copy-start.15 = (bf16[1,256,256]{2,1,0:T(8,128)(2,1)S(1)}, bf16[1,256,256]{2,1,0:T(8,128)(2,1)}, u32[]{:S(2)}) copy-start(bf16[1,256,256]{2,1,0:T(8,128)(2,1)} %get-tuple-element.12) | copy-start | bytes 393220
  142.5 14.0 %copy-start.3 = (bf16[1,16,16,4,64]{1,4,3,2,0:T(8,128)(2,1)S(1)}, bf16[1,16,16,4,64]{1,4,3,2,0:T(8,128)(2,1)}, u32[]{:S(2)}) copy-start(bf16[1,16,16,4,64]{1,4,3,2,0:T(8,128)(2,1)} %copy.142) | copy-start | bytes 393220
  156.6 10.3 %copy-start.22 = (f32[16,4,16]{2,1,0:T(4,128)S(1)}, f32[16,4,16]{2,1,0:T(4,128)}, u32[]{:S(2)}) copy-start(f32[16,4,16]{2,1,0:T(4,128)} %copy-done.21) | copy-start | bytes 12292
  156.6 10.3 %copy-start.25 = (f32[16,4,16]{2,1,0:T(4,128)S(1)}, f32[16,4,16]{2,1,0:T(4,128)}, u32[]{:S(2)}) copy-start(f32[16,4,16]{2,1,0:T(4,128)} %copy-done.24) | copy-start | bytes 12292
  166.9 2.9 %copy-start.27 = (f32[256,4]{0,1:T(4,128)S(1)}, f32[256,4]{0,1:T(4,128)}, u32[]{:S(2)}) copy-start(f32[256,4]{0,1:T(4,128)} %stack_reshape.13) | copy-start | bytes 12292
  166.9 2.9 %copy-start.28 = (f32[256,4]{0,1:T(4,128)S(1)}, f32[256,4]{0,1:T(4,128)}, u32[]{:S(2)}) copy-start(f32[256,4]{0,1:T(4,128)} %stack_reshape.14) | copy-start | bytes 12292
  166.9 3.0 %copy-start.6 = (f32[1,256,4,64]{1,3,2,0:T(8,128)S(1)}, f32[1,256,4,64]{1,3,2,0:T(8,128)}, u32[]{:S(2)}) copy-start(f32[1,256,4,64]{1,3,2,0:T(8,128)} %copy.148) | copy-start | bytes 786436
  169.3 11.7 %copy-start.1 = (bf16[256,2048]{1,0:T(8,128)(2,1)S(1)}, bf16[256,2048]{1,0:T(8,128)(2,1)}, u32[]{:S(2)}) copy-start(bf16[256,2048]{1,0:T(8,128)(2,1)} %param.5) | copy-start | bytes 3145732
  169.6 10.2 %copy-start.29 = (bf16[1024,512]{1,0:T(8,128)(2,1)S(1)}, bf16[1024,512]{1,0:T(8,128)(2,1)}, u32[]{:S(2)}) copy-start(bf16[1024,512]{1,0:T(8,128)(2,1)} %param.9) | copy-start | bytes 3145732
  (8 other events, 9.7 us)
